TPU v7x, 128 devices: a whole 4x4x4 slice. The times are simulated.
128 devices in a mesh: sp: 64 (over z, y, x), tp: 2 (over core).
Axes of the slice: x: 4, y: 4, z: 4, core: 2. Of those that a mesh axis runs over, the one named last changes fastest.
Arguments:
- features: bfloat16 [32768, 4096], P('sp', 'tp'), may hold values from -16 to 16
- weight_value: bfloat16 [4096, 1024], P(None, 'tp'), may hold values from -0.09375 to 0.09375
- weight_gate: bfloat16 [4096, 1024], P(None, 'tp'), may hold values from -0.09375 to 0.09375
- weight_out: bfloat16 [4096, 1024], P(None, 'tp'), may hold values from -0.1875 to 0.1875
- conv_taps: float32 [31, 1024], P(None, 'tp'), may hold values from -6 to 6
- norm_gain: float32 [1024], P('tp'), may hold values from 0.1 to 1.9
- out_grad: bfloat16 [32768, 4096], P('sp', 'tp'), may hold values from -16 to 16
Outputs:
- value_grad: float32 [32768, 1024], P('sp', 'tp')
- gate_grad: float32 [32768, 1024], P('sp', 'tp')
- value_wgrad: float32 [4096, 1024], P('sp', 'tp')
- gate_wgrad: float32 [4096, 1024], P('sp', 'tp')
- out_wgrad: float32 [4096, 1024], P('sp', 'tp')
- taps_grad: float32 [31, 1024], P(None, 'tp')
- gain_grad: float32 [1024], P('tp')
All inputs are finite; a program needn't handle non-finite values.
Results may differ from a plain program's by a relative error of at most 0.0057.
Values may be sent and summed in bfloat16 or wider, within the bound.
A program may use at most 192 MiB of HBM per device.

v0:
```python
import jax
import jax.numpy as jnp
from jax import lax
from jax.sharding import Mesh
from jax.sharding import PartitionSpec as P

SP = ("sp_0", "sp_1", "sp_2")
NORM_EPS = 1e-05


def sum_by_axis(running, axes):
    for axis in axes:
        running = lax.psum_scatter(running, axis, scatter_dimension=0, tiled=True)
    return running


def in_one_piece(arrays, axis, dim, along):
    ends, at = ([], 0)
    for a in arrays[:-1]:
        at += a.shape[along]
        ends.append(at)
    both = jnp.concatenate(arrays, axis=along)
    return tuple(jnp.split(lax.all_gather(both, axis, axis=dim, tiled=True), ends, axis=along))


def with_halo(block, sides, width):
    for axis, dim in sides:
        count = lax.axis_size(axis)
        forward = [(i, i + 1) for i in range(count - 1)]
        backward = [(target, source) for source, target in forward]
        low = lax.ppermute(
            lax.slice_in_dim(block, block.shape[dim] - width, None, axis=dim), axis, forward
        )
        high = lax.ppermute(lax.slice_in_dim(block, 0, width, axis=dim), axis, backward)
        block = jnp.concatenate([low, block, high], axis=dim)
    return block


def from_everyone(x, axis):
    devices = lax.axis_size(axis)
    return lax.all_to_all(jnp.broadcast_to(x[None], (devices, *x.shape)), axis, 0, 0, tiled=True)


def of_everyone(x, axis):
    return from_everyone(x, axis).sum(axis=0)


def packed_total(arrays, axis):
    vector, at, finished = (jnp.concatenate([a.reshape(-1) for a in arrays]), 0, [])
    running = of_everyone(vector, axis)
    for a in arrays:
        finished.append(running[at : at + a.size].reshape(a.shape))
        at += a.size
    return tuple(finished)


def total_of_pieces(x, axis):
    return lax.all_gather(x, axis).sum(0)


def make_term(left_rows, right_rows):
    return lax.dot_general(
        left_rows, right_rows, (((0,), (0,)), ((), ())), preferred_element_type=jnp.float32
    )


def out_weight_sum(whole_cotangent, act_half):
    term = make_term(whole_cotangent, act_half).astype(jnp.bfloat16)
    return sum_by_axis(term, SP).astype(jnp.float32)


def on_device(features, weight_value, weight_gate, weight_out, conv_taps, norm_gain, out_grad):
    whole_inputs, whole_cotangent = in_one_piece((features, out_grad), "tp", 1, 0)
    value_half = jnp.dot(whole_inputs, weight_value, preferred_element_type=jnp.float32).astype(
        jnp.bfloat16
    )
    gate_half = jnp.dot(whole_inputs, weight_gate, preferred_element_type=jnp.float32).astype(
        jnp.bfloat16
    )
    value_half, gate_half = lax.optimization_barrier((value_half, gate_half))
    value_pre = value_half.astype(jnp.float32)
    gate_pre = gate_half.astype(jnp.float32)
    gate_sig = jax.nn.sigmoid(gate_pre)
    mixed_half = lax.optimization_barrier((value_pre * gate_sig).astype(jnp.bfloat16))
    tap_count = conv_taps.shape[0]
    half_width = tap_count // 2
    row_count = mixed_half.shape[0]
    channels = mixed_half.shape[1] * lax.axis_size("tp")
    extended = with_halo(mixed_half, ((SP, 0),), half_width).astype(jnp.float32)
    conv_out = jnp.zeros(mixed_half.shape, jnp.float32)
    for offset in range(tap_count):
        conv_out = conv_out + conv_taps[offset] * extended[offset : offset + row_count]
    row_sum, row_square = packed_total(
        (jnp.sum(conv_out, axis=-1), jnp.sum(conv_out * conv_out, axis=-1)), "tp"
    )
    mean_row = row_sum[:, None] / channels
    var_row = row_square[:, None] / channels - mean_row * mean_row
    inv_std = lax.rsqrt(var_row + NORM_EPS)
    normed = (conv_out - mean_row) * inv_std
    pre_act = normed * norm_gain
    act_sig = jax.nn.sigmoid(pre_act)
    act_half = (pre_act * act_sig).astype(jnp.bfloat16)
    act_grad = jnp.dot(whole_cotangent, weight_out, preferred_element_type=jnp.float32)
    pre_grad = act_grad * act_sig * (1.0 + pre_act * (1.0 - act_sig))
    gain_part = jnp.sum(pre_grad * normed, axis=0)
    norm_grad = pre_grad * norm_gain
    first_sum, second_sum = packed_total(
        (jnp.sum(norm_grad, axis=-1), jnp.sum(norm_grad * normed, axis=-1)), "tp"
    )
    first_mom = first_sum[:, None] / channels
    second_mom = second_sum[:, None] / channels
    conv_grad = inv_std * (norm_grad - first_mom - normed * second_mom)
    grad_ext = with_halo(conv_grad, ((SP, 0),), half_width)
    mixed_grad = jnp.zeros(conv_grad.shape, jnp.float32)
    taps_rows = []
    for offset in range(tap_count):
        begin = 2 * half_width - offset
        mixed_grad = mixed_grad + conv_taps[offset] * grad_ext[begin : begin + row_count]
        taps_rows.append(jnp.sum(conv_grad * extended[offset : offset + row_count], axis=0))
    small = lax.psum(jnp.concatenate([jnp.stack(taps_rows), gain_part[None]], axis=0), SP)
    taps_grad, gain_grad = (small[:tap_count], small[tap_count])
    value_grad = mixed_grad * gate_sig
    gate_grad = mixed_grad * value_pre * gate_sig * (1.0 - gate_sig)
    value_low = value_grad.astype(jnp.bfloat16)
    gate_low = gate_grad.astype(jnp.bfloat16)
    out_wgrad = out_weight_sum(whole_cotangent, act_half)
    both_low = jnp.concatenate([value_low, gate_low], axis=1)
    joined = sum_by_axis(make_term(whole_inputs, both_low).astype(jnp.bfloat16), SP)
    joined = joined.astype(jnp.float32)
    split_at = value_low.shape[1]
    value_wgrad = joined[:, :split_at]
    gate_wgrad = joined[:, split_at:]
    return (value_grad, gate_grad, value_wgrad, gate_wgrad, out_wgrad, taps_grad, gain_grad)


def solution(mesh):
    split = Mesh(mesh.devices.reshape(4, 4, 4, mesh.shape["tp"]), ("sp_0", "sp_1", "sp_2", "tp"))
    return jax.shard_map(
        on_device,
        mesh=split,
        in_specs=(
            P(SP, "tp"),
            P(None, "tp"),
            P(None, "tp"),
            P(None, "tp"),
            P(None, "tp"),
            P("tp"),
            P(SP, "tp"),
        ),
        out_specs=(
            P(SP, "tp"),
            P(SP, "tp"),
            P(SP, "tp"),
            P(SP, "tp"),
            P(SP, "tp"),
            P(None, "tp"),
            P("tp"),
        ),
        check_vma=False,
    )
```

profile of v0, /device:TPU:0, one launch (start us, length us, event | category | flops | bytes accessed | tf_op | source)
XLA Modules:
  0.0 446.9 jit_solution(9746865256533950565)
XLA Ops:
  7.2 0.0 all-gather.2.cloned.1.call-start
  7.2 4.8 %pad_maximum_fusion = bf16[1024,2048]{1,0:T(8,128)(2,1)} fusion(bf16[512,2048]{1,0:T(8,128)(2,1)} %param.13, bf16[512,2048]{1,0:T(8,128)(2,1)} %param.7), kind=kLoop, calls=%fused_computation.30 | loop fusion | flops 8388608 | bytes 8388608 | tf_op jit(solution)/shard_map/concatenate | solution.py:22
  12.0 0.0 reduce-scatter.13.cloned.1.call-start
  12.1 0.8 copy-done.1
  12.9 24.3 %all-gather.2.cloned.1.call-done = bf16[1024,4096]{1,0:T(8,128)(2,1)} async-done(((bf16[1024,2048]{1,0:T(8,128)(2,1)}), bf16[1024,4096]{1,0:T(8,128)(2,1)}) %all-gather.2.cloned.1.call-update) | async-done | bytes 8388624 | tf_op jit(solution)/shard_map/all_gather | solution.py:23
  37.2 5.9 %fusion.14 = bf16[512,512]{1,0:T(8,128)(2,1)S(1)} fusion(bf16[4096,512]{1,0:T(8,128)(2,1)} %param.8, bf16[1024,4096]{1,0:T(8,128)(2,1)} %all-gather.2.cloned.1.call-done), kind=kOutput, calls=%fused_computation.43 | convolution fusion | flops 2147745792 | bytes 8912896 | tf_op jit(solution)/shard_map/dot_general | solution.py:74
  43.1 1.1 copy-done.4
  44.2 2.3 fusion.17
  46.6 0.3 fusion.20
  46.9 3.5 collective-permute-start
  50.4 1.3 collective-permute-start.1
  51.7 0.1 collective-permute-done
  51.8 4.2 collective-permute-done.1
  56.0 0.2 maximum_convert_fusion
  56.2 5.1 %fusion.121 = (f32[512]{0:T(512)S(1)}, f32[512]{0:T(512)S(1)}, f32[512,512]{1,0:T(8,128)S(1)}) fusion(f32[542,512]{1,0:T(8,128)S(1)} %maximum_convert_fusion, f32[512]{0:T(512)S(1)} %bitcast.127, f32[512]{0:T(512)S(1)} %bitcast.129, f32[512]{0:T(512)S(1)} %bitcast.71, f32[512]{0:T(512)S(1)} %bitcast.73, f32[512]{0:T(512)S(1)} %bitcast.75, ...), kind=kLoop, calls=%fused_computation.219 | loop fusion | flops 16776192 | bytes 33622016 | tf_op jit(solution)/shard_map/reduce_sum | solution.py:94
  61.3 3.7 all_to_all.12
  65.0 6.7 %convolution_convert_fusion.1 = bf16[4096,512]{1,0:T(8,128)(2,1)} fusion(bf16[1024,4096]{1,0:T(8,128)(2,1)} %all-gather.2.cloned.1.call-done, f32[512,512]{1,0:T(8,128)S(1)} %get-tuple-element.53, f32[512]{0:T(512)S(1)} %copy-done.2, f32[512]{0:T(512)S(1)} %get-tuple-element.94, f32[512]{0:T(512)S(1)} %get-tuple-element.93), kind=kOutput, calls=%fused_computation.29 | convolution fusion | flops 2151677952 | bytes 9443328 | tf_op jit(solution)/shard_map/dot_general | solution.py:62
  71.7 0.0 reduce-scatter.13.cloned.1.call-update
  71.8 0.0 reduce-scatter.7.cloned.1.call-start
  71.8 7.1 %multiply_reduce_fusion = (f32[512]{0:T(512)S(1)}, f32[512]{0:T(512)S(1)}, f32[512]{0:T(512)S(1)}, f32[512,512]{1,0:T(8,128)}) fusion(f32[512,512]{1,0:T(8,128)S(1)} %get-tuple-element.53, f32[512]{0:T(512)S(1)} %get-tuple-element.94, f32[512]{0:T(512)S(1)} %get-tuple-element.93, f32[512]{0:T(512)S(1)} %copy-done.2, bf16[4096,512]{1,0:T(8,128)(2,1)} %param.10, ...), kind=kOutput, calls=%fused_computation.164 | convolution fusion | flops 2151938560 | bytes 10498048 | tf_op jit(solution)/shard_map/dot_general | solution.py:103
  79.0 3.7 all_to_all.13
  82.7 4.2 multiply_reduce_fusion.1
  86.9 1.3 collective-permute-start.2
  88.2 4.5 %collective-permute-start.3 = (f32[15,512]{1,0:T(8,128)S(1)}, f32[15,512]{1,0:T(8,128)S(1)}, u32[]{:S(2)}, u32[]{:S(2)}) collective-permute-start(f32[15,512]{1,0:T(8,128)S(1)} %get-tuple-element.55), channel_id=1, source_target_pairs={{0,2},{2,4},{4,6},{6,8},{8,10},{10,12},{12,14},{14,16},{16,18},{18... | collective-permute-start | bytes 92168 | tf_op jit(solution)/shard_map/ppermute | solution.py:31
  92.8 1.6 collective-permute-done.3
  94.4 5.9 %fusion.122 = (bf16[512,512]{1,0:T(8,128)(2,1)}, f32[512,512]{1,0:T(8,128)}, f32[512,512]{1,0:T(8,128)}) fusion(bf16[512,512]{1,0:T(8,128)(2,1)S(1)} %fusion.17, f32[512,512]{1,0:T(8,128)S(1)} %get-tuple-element.47, f32[15,512]{1,0:T(8,128)S(1)} %collective-permute-done.3, f32[512]{0:T(512)S(1)} %bitcast.128, f32[512]{0:T(512)S(1)} %bitcast.130, ...), kind=kLoop, calls=%fused_computation.220 | loop fusion | flops 25427968 | bytes 4319232 | tf_op jit(solution)/shard_map/convert_element_type | solution.py:124
  100.2 2.6 fusion.125
  102.8 10.2 %convolution_convert_fusion = bf16[4096,1024]{1,0:T(8,128)(2,1)} fusion(bf16[1024,4096]{1,0:T(8,128)(2,1)} %all-gather.2.cloned.1.call-done, bf16[512,512]{1,0:T(8,128)(2,1)S(1)} %get-tuple-element.51, bf16[512,512]{1,0:T(8,128)(2,1)} %get-tuple-element.48), kind=kOutput, calls=%fused_computation | convolution fusion | flops 4301258752 | bytes 13631488 | tf_op jit(solution)/shard_map/dot_general | solution.py:62
  113.0 0.0 reduce-scatter.15.cloned.1.call-start
  113.0 10.5 %reduce-scatter.13.cloned.1.call-done = bf16[1024,512]{1,0:T(8,128)(2,1)} async-done(((bf16[4096,512]{1,0:T(8,128)(2,1)}), bf16[1024,512]{1,0:T(8,128)(2,1)}) %reduce-scatter.13.cloned.1.call-update) | async-done | bytes 1048592 | tf_op jit(solution)/shard_map/reduce_scatter | solution.py:13
  123.6 0.0 reduce-scatter.15.cloned.1.call-update
  123.6 0.0 reduce-scatter.9.cloned.1.call-start
  123.7 82.9 %reduce-scatter.7.cloned.1.call-done = bf16[1024,1024]{1,0:T(8,128)(2,1)} async-done(((bf16[4096,1024]{1,0:T(8,128)(2,1)}), bf16[1024,1024]{1,0:T(8,128)(2,1)}) %reduce-scatter.7.cloned.1.call-update) | async-done | bytes 2097168 | tf_op jit(solution)/shard_map/reduce_scatter | solution.py:13
  206.6 0.0 reduce-scatter.9.cloned.1.call-update
  206.6 0.0 all-reduce.2.cloned.1.call-start
  206.7 1.7 multiply_reduce_fusion.2
  208.4 2.5 concatenate.60
  210.9 0.0 reduce-scatter.17.cloned.1.call-start
  211.0 21.2 %reduce-scatter.15.cloned.1.call-done = bf16[256,512]{1,0:T(8,128)(2,1)} async-done(((bf16[1024,512]{1,0:T(8,128)(2,1)}), bf16[256,512]{1,0:T(8,128)(2,1)}) %reduce-scatter.15.cloned.1.call-update) | async-done | bytes 262160 | tf_op jit(solution)/shard_map/reduce_scatter | solution.py:13
  232.2 0.0 reduce-scatter.11.cloned.1.call-start
  232.3 31.7 %reduce-scatter.9.cloned.1.call-done = bf16[256,1024]{1,0:T(8,128)(2,1)} async-done(((bf16[1024,1024]{1,0:T(8,128)(2,1)}), bf16[256,1024]{1,0:T(8,128)(2,1)}) %reduce-scatter.9.cloned.1.call-update) | async-done | bytes 524304 | tf_op jit(solution)/shard_map/reduce_scatter | solution.py:13
  264.0 128.1 %all-reduce.2.cloned.1.call-done = f32[32,512]{1,0:T(8,128)} async-done(((f32[32,512]{1,0:T(8,128)}), f32[32,512]{1,0:T(8,128)}) %all-reduce.2.cloned.1.call-update) | async-done | bytes 65552 | tf_op jit(solution)/shard_map/psum | solution.py:120
  392.1 1.3 slice.602
  393.4 19.8 %reduce-scatter.17.cloned.1.call-done = bf16[64,512]{1,0:T(8,128)(2,1)} async-done(((bf16[256,512]{1,0:T(8,128)(2,1)}), bf16[64,512]{1,0:T(8,128)(2,1)}) %reduce-scatter.17.cloned.1.call-update) | async-done | bytes 65552 | tf_op jit(solution)/shard_map/reduce_scatter | solution.py:13
  413.2 1.5 convert_element_type.51
  414.7 22.3 %reduce-scatter.11.cloned.1.call-done = bf16[64,1024]{1,0:T(8,128)(2,1)} async-done(((bf16[256,1024]{1,0:T(8,128)(2,1)}), bf16[64,1024]{1,0:T(8,128)(2,1)}) %reduce-scatter.11.cloned.1.call-update) | async-done | bytes 131088 | tf_op jit(solution)/shard_map/reduce_scatter | solution.py:13
  437.0 1.6 fusion.129
  438.6 1.5 copy.23
  (26 shorter events, 0.3 us)
Async XLA Ops:
  7.2 30.0 %all-gather.2.cloned.1.call-start = ((), (), s32[]{:S(2)}) async-start(), calls=%async_computation.8 | async-start | bytes 12582912 | tf_op jit(solution)/shard_map/all_gather | solution.py:23
  12.0 0.8 copy-start.1
  12.0 111.6 %reduce-scatter.13.cloned.1.call-start = ((), (), s32[]{:S(2)}) async-start(), calls=%async_computation.12 | async-start | bytes 5242880 | tf_op jit(solution)/shard_map/reduce_scatter | solution.py:13
  37.2 5.9 %copy-start.3 = (bf16[1024,4096]{1,0:T(8,128)(2,1)S(1)}, bf16[1024,4096]{1,0:T(8,128)(2,1)}, u32[]{:S(2)}) copy-start(bf16[1024,4096]{1,0:T(8,128)(2,1)} %all-gather.2.cloned.1.call-done) | copy-start | bytes 25165828
  37.2 7.0 %copy-start.4 = (bf16[4096,512]{1,0:T(8,128)(2,1)S(1)}, bf16[4096,512]{1,0:T(8,128)(2,1)}, u32[]{:S(2)}) copy-start(bf16[4096,512]{1,0:T(8,128)(2,1)} %param.9) | copy-start | bytes 12582916
  46.9 4.9 %collective-permute-start = (bf16[15,512]{1,0:T(8,128)(2,1)S(1)}, bf16[15,512]{1,0:T(8,128)(2,1)S(1)}, u32[]{:S(2)}, u32[]{:S(2)}) collective-permute-start(bf16[15,512]{1,0:T(8,128)(2,1)S(1)} %get-tuple-element.56), channel_id=1, source_target_pairs={{0,2},{2,4},{4,6},{6,8},{8,10},{10,12},{12,14},{14,16},{16,18},{18... | collective-permute-start | bytes 46088 | tf_op jit(solution)/shard_map/ppermute | solution.py:31
  50.4 5.6 %collective-permute-start.1 = (bf16[15,512]{1,0:T(8,128)(2,1)S(1)}, bf16[15,512]{1,0:T(8,128)(2,1)S(1)}, u32[]{:S(2)}, u32[]{:S(2)}) collective-permute-start(bf16[15,512]{1,0:T(8,128)(2,1)S(1)} %get-tuple-element.57), channel_id=1, source_target_pairs={{2,0},{4,2},{6,4},{8,6},{10,8},{12,10},{14,12},{16,14},{18,16},{20... | collective-permute-start | bytes 46088 | tf_op jit(solution)/shard_map/ppermute | solution.py:34
  56.2 8.9 %copy-start.2 = (f32[512]{0:T(512)S(1)}, f32[512]{0:T(512)}, u32[]{:S(2)}) copy-start(f32[512]{0:T(512)} %param.12) | copy-start | bytes 6148
  61.2 10.6 %copy-start = (f32[512,512]{1,0:T(8,128)}, f32[512,512]{1,0:T(8,128)S(1)}, u32[]{:S(2)}) copy-start(f32[512,512]{1,0:T(8,128)S(1)} %get-tuple-element.53) | copy-start | bytes 3145732
  71.8 134.8 %reduce-scatter.7.cloned.1.call-start = ((), (), s32[]{:S(2)}) async-start(), calls=%async_computation.9 | async-start | bytes 10485760 | tf_op jit(solution)/shard_map/reduce_scatter | solution.py:13
  86.9 5.9 %collective-permute-start.2 = (f32[15,512]{1,0:T(8,128)S(1)}, f32[15,512]{1,0:T(8,128)S(1)}, u32[]{:S(2)}, u32[]{:S(2)}) collective-permute-start(f32[15,512]{1,0:T(8,128)S(1)} %get-tuple-element.54), channel_id=1, source_target_pairs={{2,0},{4,2},{6,4},{8,6},{10,8},{12,10},{14,12},{16,14},{18,16},{20... | collective-permute-start | bytes 92168 | tf_op jit(solution)/shard_map/ppermute | solution.py:34
  88.2 6.1 %collective-permute-start.3 = (f32[15,512]{1,0:T(8,128)S(1)}, f32[15,512]{1,0:T(8,128)S(1)}, u32[]{:S(2)}, u32[]{:S(2)}) collective-permute-start(f32[15,512]{1,0:T(8,128)S(1)} %get-tuple-element.55), channel_id=1, source_target_pairs={{0,2},{2,4},{4,6},{6,8},{8,10},{10,12},{12,14},{14,16},{16,18},{18... | collective-permute-start | bytes 92168 | tf_op jit(solution)/shard_map/ppermute | solution.py:31
  113.0 119.2 %reduce-scatter.15.cloned.1.call-start = ((), (), s32[]{:S(2)}) async-start(), calls=%async_computation.13 | async-start | bytes 1310720 | tf_op jit(solution)/shard_map/reduce_scatter | solution.py:13
  123.6 140.4 %reduce-scatter.9.cloned.1.call-start = ((), (), s32[]{:S(2)}) async-start(), calls=%async_computation.10 | async-start | bytes 2621440 | tf_op jit(solution)/shard_map/reduce_scatter | solution.py:13
  206.6 185.5 %all-reduce.2.cloned.1.call-start = ((), (), s32[]{:S(2)}) async-start(), calls=%async_computation.15 | async-start | bytes 131072 | tf_op jit(solution)/shard_map/psum | solution.py:120
  210.9 202.3 %reduce-scatter.17.cloned.1.call-start = ((), (), s32[]{:S(2)}) async-start(), calls=%async_computation.14 | async-start | bytes 327680 | tf_op jit(solution)/shard_map/reduce_scatter | solution.py:13
  232.2 204.7 %reduce-scatter.11.cloned.1.call-start = ((), (), s32[]{:S(2)}) async-start(), calls=%async_computation.11 | async-start | bytes 655360 | tf_op jit(solution)/shard_map/reduce_scatter | solution.py:13
Sparse Core Ops, SparseCore 0:
  12.1 25.0 all-gather.1
  71.9 51.6 reduce-scatter.12
  126.1 80.4 reduce-scatter.6
  208.8 23.3 reduce-scatter.14
  234.5 29.4 reduce-scatter.8
  269.1 123.0 all-reduce.1
  394.5 18.6 reduce-scatter.16
  415.6 21.3 reduce-scatter.10
where the time goes:
time: 448 us; the launch traced here: 447 us
  waiting for transfers between devices  347 us (77%)
  matrix products  32.2 us (7%)
  other arithmetic  26.2 us (6%)
  between operations  14.3 us (3%)
  starting transfers between devices  10.9 us (2%)
  local copies, waits for them, and re-layouts  8.86 us (2%)
  blocking collectives  7.42 us (2%)
    reduce_scatter x6, waiting for transfers between devices, sum_by_axis(): running = lax.psum_scatter(running, axis, scatter_dimension=0, tiled=True)  188 us
    psum x1, waiting for transfers between devices, on_device(): lax.psum(jnp.concatenate([jnp.stack(taps_rows), gain_part[None]], axis=0)...  128 us
    all_gather x1, waiting for transfers between devices, in_one_piece(): lax.all_gather(both, axis, axis=dim, tiled=True)  24.3 us
    dot_general x2, matrix products, make_term(): lax.dot_general(left_rows, right_rows, (((0,), (0,)), ((), ())), preferre...  16.9 us
  transfers between devices with their start and end apart: 12, of which 11 were waited for; matrix products, arithmetic and copies ran while one was open for 8% of the time, Pallas kernels for 0%

commit v1 on v0

--- a/solution.py
+++ b/solution.py
@@ -117,7 +117,9 @@
         begin = 2 * half_width - offset
         mixed_grad = mixed_grad + conv_taps[offset] * grad_ext[begin : begin + row_count]
         taps_rows.append(jnp.sum(conv_grad * extended[offset : offset + row_count], axis=0))
-    small = lax.psum(jnp.concatenate([jnp.stack(taps_rows), gain_part[None]], axis=0), SP)
+    value = jnp.concatenate([jnp.stack(taps_rows), gain_part[None]], axis=0)
+    parts = lax.all_gather(value, SP, axis=0, tiled=False)
+    small = parts.sum(axis=0)
     taps_grad, gain_grad = (small[:tap_count], small[tap_count])
     value_grad = mixed_grad * gate_sig
     gate_grad = mixed_grad * value_pre * gate_sig * (1.0 - gate_sig)

time: 448 us -> 389 us (0.87)
  waiting for transfers between devices: 347 us -> 288 us
    psum x1 -> x0, waiting for transfers between devices: 128 us -> none  [on_device(): lax.psum(jnp.concatenate([jnp.stack(taps_rows), gain_part[None]], axis=0)...]
    all_gather x0 -> x1, waiting for transfers between devices: none -> 71.6 us  [on_device(): parts = lax.all_gather(value, SP, axis=0, tiled=False)]
  transfers between devices with their start and end apart: 12 -> 12, of which waited for: 11 -> 11; matrix products, arithmetic and copies ran while one was open for 8% -> 10% of each run, Pallas kernels for 0% -> 0%
where the time goes in v1:
time: 389 us; the launch traced here: 388 us
  waiting for transfers between devices  288 us (74%)
  matrix products  32.2 us (8%)
  other arithmetic  28.7 us (7%)
  between operations  14.4 us (4%)
  starting transfers between devices  10.9 us (3%)
  blocking collectives  7.42 us (2%)
  local copies, waits for them, and re-layouts  6.68 us (2%)
    reduce_scatter x6, waiting for transfers between devices, sum_by_axis(): running = lax.psum_scatter(running, axis, scatter_dimension=0, tiled=True)  186 us
    all_gather x1, waiting for transfers between devices, on_device(): parts = lax.all_gather(value, SP, axis=0, tiled=False)  71.6 us
    all_gather x1, waiting for transfers between devices, in_one_piece(): lax.all_gather(both, axis, axis=dim, tiled=True)  24.3 us
    dot_general x2, matrix products, make_term(): lax.dot_general(left_rows, right_rows, (((0,), (0,)), ((), ())), preferre...  16.9 us
    ppermute x2, starting transfers between devices, with_halo(): lax.ppermute(lax.slice_in_dim(block, block.shape[dim] - width, None, axis...  8.03 us
  transfers between devices with their start and end apart: 12, of which 11 were waited for; matrix products, arithmetic and copies ran while one was open for 10% of the time, Pallas kernels for 0%

profile of v1, /device:TPU:0, one launch (start us, length us, event | category | flops | bytes accessed | tf_op | source)
XLA Modules:
  0.0 388.4 jit_solution(4725386152980991302)
XLA Ops:
  7.2 0.0 all-gather.4.cloned.1.call-start
  7.2 4.8 %pad_maximum_fusion = bf16[1024,2048]{1,0:T(8,128)(2,1)} fusion(bf16[512,2048]{1,0:T(8,128)(2,1)} %param.13, bf16[512,2048]{1,0:T(8,128)(2,1)} %param.7), kind=kLoop, calls=%fused_computation.30 | loop fusion | flops 8388608 | bytes 8388608 | tf_op jit(solution)/shard_map/concatenate | solution.py:22
  12.0 0.0 reduce-scatter.13.cloned.1.call-start
  12.1 0.8 copy-done.2
  12.9 24.3 %all-gather.4.cloned.1.call-done = bf16[1024,4096]{1,0:T(8,128)(2,1)} async-done(((bf16[1024,2048]{1,0:T(8,128)(2,1)}), bf16[1024,4096]{1,0:T(8,128)(2,1)}) %all-gather.4.cloned.1.call-update) | async-done | bytes 8388624 | tf_op jit(solution)/shard_map/all_gather | solution.py:23
  37.2 5.9 %fusion.14 = bf16[512,512]{1,0:T(8,128)(2,1)S(1)} fusion(bf16[4096,512]{1,0:T(8,128)(2,1)} %param.8, bf16[1024,4096]{1,0:T(8,128)(2,1)} %all-gather.4.cloned.1.call-done), kind=kOutput, calls=%fused_computation.43 | convolution fusion | flops 2147745792 | bytes 8912896 | tf_op jit(solution)/shard_map/dot_general | solution.py:74
  43.1 1.1 copy-done.5
  44.2 2.3 fusion.17
  46.6 0.3 fusion.20
  46.9 3.5 collective-permute-start
  50.4 1.3 collective-permute-start.1
  51.7 0.1 collective-permute-done
  51.8 4.2 %collective-permute-done.1 = bf16[15,512]{1,0:T(8,128)(2,1)S(1)} collective-permute-done((bf16[15,512]{1,0:T(8,128)(2,1)S(1)}, bf16[15,512]{1,0:T(8,128)(2,1)S(1)}, u32[]{:S(2)}, u32[]{:S(2)}) %collective-permute-start.1) | collective-permute-done | bytes 15392 | tf_op jit(solution)/shard_map/ppermute | solution.py:34
  56.0 0.2 maximum_convert_fusion
  56.2 5.1 %fusion.121 = (f32[512]{0:T(512)S(1)}, f32[512]{0:T(512)S(1)}, f32[512,512]{1,0:T(8,128)S(1)}) fusion(f32[542,512]{1,0:T(8,128)S(1)} %maximum_convert_fusion, f32[512]{0:T(512)S(1)} %bitcast.129, f32[512]{0:T(512)S(1)} %bitcast.131, f32[512]{0:T(512)S(1)} %bitcast.73, f32[512]{0:T(512)S(1)} %bitcast.75, f32[512]{0:T(512)S(1)} %bitcast.77, ...), kind=kLoop, calls=%fused_computation.219 | loop fusion | flops 16776192 | bytes 33622016 | tf_op jit(solution)/shard_map/reduce_sum | solution.py:94
  61.3 3.7 all_to_all.12
  65.0 6.7 %convolution_convert_fusion.1 = bf16[4096,512]{1,0:T(8,128)(2,1)} fusion(bf16[1024,4096]{1,0:T(8,128)(2,1)} %all-gather.4.cloned.1.call-done, f32[512,512]{1,0:T(8,128)S(1)} %get-tuple-element.53, f32[512]{0:T(512)S(1)} %copy-done.3, f32[512]{0:T(512)S(1)} %get-tuple-element.94, f32[512]{0:T(512)S(1)} %get-tuple-element.93), kind=kOutput, calls=%fused_computation.29 | convolution fusion | flops 2151677952 | bytes 9443328 | tf_op jit(solution)/shard_map/dot_general | solution.py:62
  71.7 0.0 reduce-scatter.13.cloned.1.call-update
  71.8 0.0 reduce-scatter.7.cloned.1.call-start
  71.8 7.1 %multiply_reduce_fusion = (f32[512]{0:T(512)S(1)}, f32[512]{0:T(512)S(1)}, f32[512]{0:T(512)S(1)}, f32[512,512]{1,0:T(8,128)}) fusion(f32[512,512]{1,0:T(8,128)S(1)} %get-tuple-element.53, f32[512]{0:T(512)S(1)} %get-tuple-element.94, f32[512]{0:T(512)S(1)} %get-tuple-element.93, f32[512]{0:T(512)S(1)} %copy-done.3, bf16[4096,512]{1,0:T(8,128)(2,1)} %param.10, ...), kind=kOutput, calls=%fused_computation.164 | convolution fusion | flops 2151938560 | bytes 10498048 | tf_op jit(solution)/shard_map/dot_general | solution.py:103
  79.0 3.7 all_to_all.13
  82.7 4.2 %multiply_reduce_fusion.1 = (f32[512]{0:T(512)S(1)}, f32[512]{0:T(512)S(1)}, f32[512]{0:T(512)S(1)}, f32[512]{0:T(512)S(1)}, f32[512]{0:T(512)S(1)}, /*index=5*/...) fusion(f32[542,512]{1,0:T(8,128)S(1)} %maximum_convert_fusion, ...), kind=kLoop, calls=%fused_computation.165 | loop fusion | flops 11262976 | bytes 22067200 | tf_op jit(solution)/shard_map/reduce_sum | solution.py:119
  86.9 1.3 collective-permute-start.2
  88.2 4.5 %collective-permute-start.3 = (f32[15,512]{1,0:T(8,128)S(1)}, f32[15,512]{1,0:T(8,128)S(1)}, u32[]{:S(2)}, u32[]{:S(2)}) collective-permute-start(f32[15,512]{1,0:T(8,128)S(1)} %get-tuple-element.55), channel_id=1, source_target_pairs={{0,2},{2,4},{4,6},{6,8},{8,10},{10,12},{12,14},{14,16},{16,18},{18... | collective-permute-start | bytes 92168 | tf_op jit(solution)/shard_map/ppermute | solution.py:31
  92.8 1.6 collective-permute-done.3
  94.4 5.9 %fusion.122 = (bf16[512,512]{1,0:T(8,128)(2,1)}, f32[512,512]{1,0:T(8,128)}, f32[512,512]{1,0:T(8,128)}) fusion(bf16[512,512]{1,0:T(8,128)(2,1)S(1)} %fusion.17, f32[512,512]{1,0:T(8,128)S(1)} %get-tuple-element.47, f32[15,512]{1,0:T(8,128)S(1)} %collective-permute-done.3, f32[512]{0:T(512)S(1)} %bitcast.130, f32[512]{0:T(512)S(1)} %bitcast.132, ...), kind=kLoop, calls=%fused_computation.220 | loop fusion | flops 25427968 | bytes 4319232 | tf_op jit(solution)/shard_map/convert_element_type | solution.py:126
  100.2 2.6 fusion.125
  102.8 10.2 %convolution_convert_fusion = bf16[4096,1024]{1,0:T(8,128)(2,1)} fusion(bf16[1024,4096]{1,0:T(8,128)(2,1)} %all-gather.4.cloned.1.call-done, bf16[512,512]{1,0:T(8,128)(2,1)S(1)} %get-tuple-element.51, bf16[512,512]{1,0:T(8,128)(2,1)} %get-tuple-element.48), kind=kOutput, calls=%fused_computation | convolution fusion | flops 4301258752 | bytes 13631488 | tf_op jit(solution)/shard_map/dot_general | solution.py:62
  113.0 0.0 reduce-scatter.15.cloned.1.call-start
  113.0 10.5 %reduce-scatter.13.cloned.1.call-done = bf16[1024,512]{1,0:T(8,128)(2,1)} async-done(((bf16[4096,512]{1,0:T(8,128)(2,1)}), bf16[1024,512]{1,0:T(8,128)(2,1)}) %reduce-scatter.13.cloned.1.call-update) | async-done | bytes 1048592 | tf_op jit(solution)/shard_map/reduce_scatter | solution.py:13
  123.6 0.0 reduce-scatter.15.cloned.1.call-update
  123.6 0.0 reduce-scatter.9.cloned.1.call-start
  123.7 82.9 %reduce-scatter.7.cloned.1.call-done = bf16[1024,1024]{1,0:T(8,128)(2,1)} async-done(((bf16[4096,1024]{1,0:T(8,128)(2,1)}), bf16[1024,1024]{1,0:T(8,128)(2,1)}) %reduce-scatter.7.cloned.1.call-update) | async-done | bytes 2097168 | tf_op jit(solution)/shard_map/reduce_scatter | solution.py:13
  206.6 0.0 reduce-scatter.9.cloned.1.call-update
  206.6 0.0 all-gather.6.cloned.1.call-start
  206.7 1.7 multiply_reduce_fusion.2
  208.4 2.5 concatenate.60
  210.9 0.0 reduce-scatter.17.cloned.1.call-start
  211.0 21.2 %reduce-scatter.15.cloned.1.call-done = bf16[256,512]{1,0:T(8,128)(2,1)} async-done(((bf16[1024,512]{1,0:T(8,128)(2,1)}), bf16[256,512]{1,0:T(8,128)(2,1)}) %reduce-scatter.15.cloned.1.call-update) | async-done | bytes 262160 | tf_op jit(solution)/shard_map/reduce_scatter | solution.py:13
  232.2 0.0 reduce-scatter.11.cloned.1.call-start
  232.3 31.7 %reduce-scatter.9.cloned.1.call-done = bf16[256,1024]{1,0:T(8,128)(2,1)} async-done(((bf16[1024,1024]{1,0:T(8,128)(2,1)}), bf16[256,1024]{1,0:T(8,128)(2,1)}) %reduce-scatter.9.cloned.1.call-update) | async-done | bytes 524304 | tf_op jit(solution)/shard_map/reduce_scatter | solution.py:13
  264.0 71.6 %all-gather.6.cloned.1.call-done = f32[2048,512]{1,0:T(8,128)} async-done(((f32[32,512]{1,0:T(8,128)}), f32[2048,512]{1,0:T(8,128)}) %all-gather.6.cloned.1.call-update) | async-done | bytes 4194320 | tf_op jit(solution)/shard_map/all_gather | solution.py:121
  335.6 2.5 reduce_sum.389
  338.1 0.6 slice.602
  338.7 17.5 %reduce-scatter.17.cloned.1.call-done = bf16[64,512]{1,0:T(8,128)(2,1)} async-done(((bf16[256,512]{1,0:T(8,128)(2,1)}), bf16[64,512]{1,0:T(8,128)(2,1)}) %reduce-scatter.17.cloned.1.call-update) | async-done | bytes 65552 | tf_op jit(solution)/shard_map/reduce_scatter | solution.py:13
  356.2 1.5 convert_element_type.51
  357.7 22.3 %reduce-scatter.11.cloned.1.call-done = bf16[64,1024]{1,0:T(8,128)(2,1)} async-done(((bf16[256,1024]{1,0:T(8,128)(2,1)}), bf16[64,1024]{1,0:T(8,128)(2,1)}) %reduce-scatter.11.cloned.1.call-update) | async-done | bytes 131088 | tf_op jit(solution)/shard_map/reduce_scatter | solution.py:13
  379.9 1.6 fusion.129
  (28 shorter events, 0.3 us)
Async XLA Ops:
  7.2 30.0 %all-gather.4.cloned.1.call-start = ((), (), s32[]{:S(2)}) async-start(), calls=%async_computation.8 | async-start | bytes 12582912 | tf_op jit(solution)/shard_map/all_gather | solution.py:23
  12.0 0.8 copy-start.2
  12.0 111.6 %reduce-scatter.13.cloned.1.call-start = ((), (), s32[]{:S(2)}) async-start(), calls=%async_computation.12 | async-start | bytes 5242880 | tf_op jit(solution)/shard_map/reduce_scatter | solution.py:13
  37.2 5.9 %copy-start.4 = (bf16[1024,4096]{1,0:T(8,128)(2,1)S(1)}, bf16[1024,4096]{1,0:T(8,128)(2,1)}, u32[]{:S(2)}) copy-start(bf16[1024,4096]{1,0:T(8,128)(2,1)} %all-gather.4.cloned.1.call-done) | copy-start | bytes 25165828
  37.2 7.0 %copy-start.5 = (bf16[4096,512]{1,0:T(8,128)(2,1)S(1)}, bf16[4096,512]{1,0:T(8,128)(2,1)}, u32[]{:S(2)}) copy-start(bf16[4096,512]{1,0:T(8,128)(2,1)} %param.9) | copy-start | bytes 12582916
  46.9 4.9 %collective-permute-start = (bf16[15,512]{1,0:T(8,128)(2,1)S(1)}, bf16[15,512]{1,0:T(8,128)(2,1)S(1)}, u32[]{:S(2)}, u32[]{:S(2)}) collective-permute-start(bf16[15,512]{1,0:T(8,128)(2,1)S(1)} %get-tuple-element.56), channel_id=1, source_target_pairs={{0,2},{2,4},{4,6},{6,8},{8,10},{10,12},{12,14},{14,16},{16,18},{18... | collective-permute-start | bytes 46088 | tf_op jit(solution)/shard_map/ppermute | solution.py:31
  50.4 5.6 %collective-permute-start.1 = (bf16[15,512]{1,0:T(8,128)(2,1)S(1)}, bf16[15,512]{1,0:T(8,128)(2,1)S(1)}, u32[]{:S(2)}, u32[]{:S(2)}) collective-permute-start(bf16[15,512]{1,0:T(8,128)(2,1)S(1)} %get-tuple-element.57), channel_id=1, source_target_pairs={{2,0},{4,2},{6,4},{8,6},{10,8},{12,10},{14,12},{16,14},{18,16},{20... | collective-permute-start | bytes 46088 | tf_op jit(solution)/shard_map/ppermute | solution.py:34
  56.2 8.9 %copy-start.3 = (f32[512]{0:T(512)S(1)}, f32[512]{0:T(512)}, u32[]{:S(2)}) copy-start(f32[512]{0:T(512)} %param.12) | copy-start | bytes 6148
  61.2 10.6 %copy-start = (f32[512,512]{1,0:T(8,128)}, f32[512,512]{1,0:T(8,128)S(1)}, u32[]{:S(2)}) copy-start(f32[512,512]{1,0:T(8,128)S(1)} %get-tuple-element.53) | copy-start | bytes 3145732
  71.8 134.8 %reduce-scatter.7.cloned.1.call-start = ((), (), s32[]{:S(2)}) async-start(), calls=%async_computation.9 | async-start | bytes 10485760 | tf_op jit(solution)/shard_map/reduce_scatter | solution.py:13
  86.9 5.9 %collective-permute-start.2 = (f32[15,512]{1,0:T(8,128)S(1)}, f32[15,512]{1,0:T(8,128)S(1)}, u32[]{:S(2)}, u32[]{:S(2)}) collective-permute-start(f32[15,512]{1,0:T(8,128)S(1)} %get-tuple-element.54), channel_id=1, source_target_pairs={{2,0},{4,2},{6,4},{8,6},{10,8},{12,10},{14,12},{16,14},{18,16},{20... | collective-permute-start | bytes 92168 | tf_op jit(solution)/shard_map/ppermute | solution.py:34
  88.2 6.1 %collective-permute-start.3 = (f32[15,512]{1,0:T(8,128)S(1)}, f32[15,512]{1,0:T(8,128)S(1)}, u32[]{:S(2)}, u32[]{:S(2)}) collective-permute-start(f32[15,512]{1,0:T(8,128)S(1)} %get-tuple-element.55), channel_id=1, source_target_pairs={{0,2},{2,4},{4,6},{6,8},{8,10},{10,12},{12,14},{14,16},{16,18},{18... | collective-permute-start | bytes 92168 | tf_op jit(solution)/shard_map/ppermute | solution.py:31
  113.0 119.2 %reduce-scatter.15.cloned.1.call-start = ((), (), s32[]{:S(2)}) async-start(), calls=%async_computation.13 | async-start | bytes 1310720 | tf_op jit(solution)/shard_map/reduce_scatter | solution.py:13
  123.6 140.4 %reduce-scatter.9.cloned.1.call-start = ((), (), s32[]{:S(2)}) async-start(), calls=%async_computation.10 | async-start | bytes 2621440 | tf_op jit(solution)/shard_map/reduce_scatter | solution.py:13
  206.6 129.0 %all-gather.6.cloned.1.call-start = ((), (), s32[]{:S(2)}) async-start(), calls=%async_computation.15 | async-start | bytes 4259840 | tf_op jit(solution)/shard_map/all_gather | solution.py:121
  210.9 145.2 %reduce-scatter.17.cloned.1.call-start = ((), (), s32[]{:S(2)}) async-start(), calls=%async_computation.14 | async-start | bytes 327680 | tf_op jit(solution)/shard_map/reduce_scatter | solution.py:13
  232.2 147.7 %reduce-scatter.11.cloned.1.call-start = ((), (), s32[]{:S(2)}) async-start(), calls=%async_computation.11 | async-start | bytes 655360 | tf_op jit(solution)/shard_map/reduce_scatter | solution.py:13
  338.1 43.4 %copy-start.1 = (f32[32,512]{1,0:T(8,128)}, f32[32,512]{1,0:T(8,128)S(1)}, u32[]{:S(2)}) copy-start(f32[32,512]{1,0:T(8,128)S(1)} %reduce_sum.389) | copy-start | bytes 196612
Sparse Core Ops, SparseCore 0:
  12.1 25.0 all-gather.3
  71.9 51.6 reduce-scatter.12
  126.1 80.4 reduce-scatter.6
  208.8 23.3 reduce-scatter.14
  234.5 29.4 reduce-scatter.8
  267.3 68.2 all-gather.5
  338.0 18.1 reduce-scatter.16
  358.5 21.3 reduce-scatter.10
